TPU v7x, 32 devices: a whole 2x2x4 slice. The times are simulated.
32 devices in a mesh: grp: 2 (over y), kv: 4 (over z), tp: 4 (over x, core).
Axes of the slice: x: 2, y: 2, z: 4, core: 2. Of those that a mesh axis runs over, the one named last changes fastest.
Arguments:
- tokens: bfloat16 [32, 4096], P('grp', 'kv'), parts along dimension 0, may hold values from -16 to 16
- positions: int32 [32], P(('grp', 'kv')), parts along dimension 0, may hold values from 512 to 8191
- state: float32 [32, 16, 128, 128], P(('grp', 'kv'), 'tp'), parts along dimension 0, may hold values from -3 to 3
- norm_gain: float32 [4096], P('kv'), may hold values from 0.1 to 1.9
- w_query: bfloat16 [4096, 2048], P('kv', 'tp'), may hold values from -0.09375 to 0.09375
- w_key: bfloat16 [4096, 2048], P('kv', 'tp'), may hold values from -0.09375 to 0.09375
- w_value: bfloat16 [4096, 2048], P('kv', 'tp'), may hold values from -0.09375 to 0.09375
- w_gate: bfloat16 [4096, 2048], P('kv', 'tp'), may hold values from -0.09375 to 0.09375
- w_out: bfloat16 [2048, 4096], P('tp', 'kv'), may hold values from -0.125 to 0.125
- mlp_gain: float32 [4096], P('kv'), may hold values from 0.1 to 1.9
- w_up: bfloat16 [4096, 16384], P('kv', 'tp'), may hold values from -0.09375 to 0.09375
- w_down: bfloat16 [16384, 4096], P('tp', 'kv'), may hold values from -0.046875 to 0.046875
Outputs:
- layer_out: bfloat16 [32, 4096], P('grp', 'kv'), parts along dimension 0
- new_state: float32 [32, 16, 128, 128], P(('grp', 'kv'), 'tp'), parts along dimension 0
There are 2 independent parts, one for each index of `grp`. A program takes and returns all parts, laid end to end along the dimension named above; an argument that names none is the same for every part. Nothing has to cross between parts.
All inputs are finite; a program needn't handle non-finite values.
Results may differ from a plain program's by a relative error of at most 0.007.
Values may be sent and summed in bfloat16 or wider, within the bound.
A program may use at most 64 MiB of HBM per device.

v0:
```python
import jax
import jax.numpy as jnp
from jax import lax
from jax.sharding import PartitionSpec as P

D = 4096
HEADS = 16


def turn(values, positions):
    half = values.shape[-1] // 2
    freq = 10000.0 ** (-(jnp.arange(half, dtype=jnp.float32) * 2.0) / values.shape[-1])
    angle = positions.astype(jnp.float32)[:, None, None] * freq[None, None, :]
    cosine = jnp.cos(angle)
    sine = jnp.sin(angle)
    first = values[..., :half]
    second = values[..., half:]
    return jnp.concatenate(
        [first * cosine - second * sine, first * sine + second * cosine], axis=-1
    )


def shards(
    tokens,
    positions,
    state,
    norm_gain,
    w_query,
    w_key,
    w_value,
    w_gate,
    w_out,
    mlp_gain,
    w_up,
    w_down,
):
    local_seqs, head_dev, head_size, _ = state.shape
    inputs = tokens.astype(jnp.float32)
    squares = jnp.sum(inputs * inputs, axis=1)
    normed = (inputs * norm_gain).astype(jnp.bfloat16)
    terms = jnp.stack(
        [
            jnp.dot(normed, weight, preferred_element_type=jnp.float32)
            for weight in (w_query, w_key, w_value, w_gate)
        ],
        axis=1,
    )
    summed, total_sq = (
        lax.psum_scatter(terms, "kv", scatter_dimension=0, tiled=True),
        lax.psum_scatter(squares, "kv", scatter_dimension=0, tiled=True),
    )
    scale1 = lax.rsqrt(total_sq / D + 1e-06)
    summed = (summed * scale1[:, None, None]).reshape(local_seqs, 4, head_dev, head_size)
    query = turn(summed[:, 0], positions)
    key_rows = turn(summed[:, 1], positions) * head_size ** (-0.5)
    value = summed[:, 2]
    gate = summed[:, 3]
    heads = (lax.axis_index("tp") * head_dev + jnp.arange(head_dev)).astype(jnp.float32)
    gamma = 1.0 - 2.0 ** (-5.0 - 5.0 * heads / (HEADS - 1))
    new_state = gamma[None, :, None, None] * state + key_rows[:, :, :, None] * value[:, :, None, :]
    read = jnp.einsum("bhd,bhde->bhe", query, new_state, precision=lax.Precision.HIGHEST)
    read = read * lax.rsqrt(jnp.mean(read * read, axis=-1, keepdims=True) + 1e-06)
    retained = (
        (read * jax.nn.silu(gate)).reshape(local_seqs, head_dev * head_size).astype(jnp.bfloat16)
    )
    head_terms = jnp.dot(
        lax.all_gather(retained, "kv", axis=0, tiled=True),
        w_out,
        preferred_element_type=jnp.float32,
    )
    mixed = (inputs + lax.psum(head_terms, "tp")).astype(jnp.bfloat16)
    middle = mixed.astype(jnp.float32)
    squares2 = jnp.sum(middle * middle, axis=1)
    normed2 = (middle * mlp_gain).astype(jnp.bfloat16)
    upward = jnp.dot(normed2, w_up, preferred_element_type=jnp.float32)
    up_full, total_sq2 = lax.psum((upward, squares2), "kv")
    scale2 = lax.rsqrt(total_sq2 / D + 1e-06)
    hidden = jnp.square(jax.nn.relu(up_full * scale2[:, None])).astype(jnp.bfloat16)
    down_terms = jnp.dot(hidden, w_down, preferred_element_type=jnp.float32)
    layer_out = (middle + lax.psum(down_terms, "tp")).astype(jnp.bfloat16)
    return (layer_out, new_state)


def solution(mesh):
    return jax.shard_map(
        shards,
        mesh=mesh,
        in_specs=(
            P("grp", "kv"),
            P(("grp", "kv")),
            P(("grp", "kv"), "tp", None, None),
            P("kv"),
            P("kv", "tp"),
            P("kv", "tp"),
            P("kv", "tp"),
            P("kv", "tp"),
            P("tp", "kv"),
            P("kv"),
            P("kv", "tp"),
            P("tp", "kv"),
        ),
        out_specs=(P("grp", "kv"), P(("grp", "kv"), "tp", None, None)),
        check_vma=False,
    )
```

profile of v0, /device:TPU:0, one launch (start us, length us, event | category | flops | bytes accessed | tf_op | source)
XLA Modules:
  0.0 187.9 jit_solution(12907306079230193447)
XLA Ops:
  7.2 1.6 convolution_bitcast_fusion.3
  8.8 1.5 convolution_bitcast_fusion.2
  10.3 1.5 convolution_bitcast_fusion.1
  11.8 1.5 convolution_bitcast_fusion
  13.4 0.7 pad_maximum_fusion
  14.1 0.0 all-reduce.7.cloned.1.call-start
  14.1 0.9 fusion.4
  15.0 0.7 convert_element_type.40
  15.7 0.1 multiply_cosine_fusion
  15.8 1.2 dynamic-slice
  17.7 13.5 %all-reduce.1 = f32[16]{0:T(128)S(1)} all-reduce(f32[16]{0:T(128)S(1)} %fusion.4), channel_id=3, replica_groups=mesh['grp'=2,'kv'=4,'tp'=4] {'kv'}, use_global_device_ids=true, to_apply=%region_2.0.clone | all-reduce | flops 16 | bytes 128
  31.2 0.1 fusion.19
  31.3 20.3 %all-reduce.13.cloned.1.call-done = f32[16,4,512]{2,0,1:T(8,128)} async-done(((f32[16,4,512]{2,0,1:T(8,128)}), f32[16,4,512]{2,0,1:T(8,128)}) %all-reduce.13.cloned.1.call-update) | async-done | bytes 131088
  51.6 0.9 dynamic-slice_multiply_fusion
  52.5 0.1 multiply_subtract_fusion
  52.6 0.1 pad_maximum_fusion.1
  52.7 1.6 multiply_add_fusion
  54.3 1.0 fusion.22
  55.3 0.1 multiply_reduce_fusion
  55.4 0.1 fusion.17
  55.5 13.2 %all-gather = bf16[4,4,512]{2,1,0:T(4,128)(2,1)S(1)} all-gather(bf16[1,4,512]{2,1,0:T(4,128)(2,1)S(1)} %reshape.108), channel_id=1, replica_groups=mesh['grp'=2,'kv'=4,'tp'=4] {'kv'}, dimensions={0}, use_global_device_ids=true | all-gather | bytes 20480 | tf_op jit(solution)/shard_map/all_gather | solution.py:67
  68.7 0.9 fusion.23
  69.6 0.0 all-reduce.9.cloned.1.call-start
  69.6 31.3 %all-reduce.7.cloned.1.call-done = f32[16,1024]{1,0:T(8,128)} async-done(((f32[16,1024]{1,0:T(8,128)}), f32[16,1024]{1,0:T(8,128)}) %all-reduce.7.cloned.1.call-update) | async-done | bytes 65552 | tf_op jit(solution)/shard_map/psum | solution.py:71
  101.0 1.0 fusion.7
  101.9 5.3 %fusion.9 = f32[16,4096]{1,0:T(8,128)} fusion(bf16[1024,4096]{1,0:T(8,128)(2,1)} %param.22, bf16[16,1024]{1,0:T(8,128)(2,1)S(1)} %get-tuple-element.3, f32[1024]{0:T(1024)S(1)} %copy-done.3), kind=kOutput, calls=%fused_computation.22 | convolution fusion | flops 134266880 | bytes 8687616 | tf_op jit(solution)/shard_map/dot_general | solution.py:75
  107.2 0.0 all-reduce.11.cloned.1.call-start
  107.3 11.8 %psum.30 = f32[16]{0:T(128)S(1)} all-reduce(f32[16]{0:T(128)S(1)} %get-tuple-element.2), channel_id=1, replica_groups=mesh['grp'=2,'kv'=4,'tp'=4] {'kv'}, use_global_device_ids=true, to_apply=%region_7.8 | all-reduce | flops 16 | bytes 128 | tf_op jit(solution)/shard_map/psum | solution.py:76
  119.1 23.9 %all-reduce.9.cloned.1.call-done = f32[16,4096]{1,0:T(8,128)} async-done(((f32[16,4096]{1,0:T(8,128)}), f32[16,4096]{1,0:T(8,128)}) %all-reduce.9.cloned.1.call-update) | async-done | bytes 262160 | tf_op jit(solution)/shard_map/psum | solution.py:76
  143.0 5.3 %fusion = f32[16,1024]{1,0:T(8,128)} fusion(bf16[4096,1024]{1,0:T(8,128)(2,1)} %param.23, f32[16,4096]{1,0:T(8,128)} %all-reduce.9.cloned.1.call-done, f32[16]{0:T(128)S(1)} %add_rsqrt_fusion.1), kind=kOutput, calls=%fused_computation.6 | convolution fusion | flops 134479872 | bytes 8716352 | tf_op jit(solution)/shard_map/dot_general | solution.py:79
  148.4 31.6 %all-reduce.11.cloned.1.call-done = f32[16,1024]{1,0:T(8,128)} async-done(((f32[16,1024]{1,0:T(8,128)}), f32[16,1024]{1,0:T(8,128)}) %all-reduce.11.cloned.1.call-update) | async-done | bytes 65552 | tf_op jit(solution)/shard_map/psum | solution.py:80
  179.9 1.5 fusion.8
  (21 shorter events, 0.2 us)
Async XLA Ops:
  7.2 61.5 %copy-start = (bf16[512,1024]{1,0:T(8,128)(2,1)S(1)}, bf16[512,1024]{1,0:T(8,128)(2,1)}, u32[]{:S(2)}) copy-start(bf16[512,1024]{1,0:T(8,128)(2,1)} %param.20) | copy-start | bytes 3145732
  7.2 93.8 %copy-start.2 = (bf16[16,1024]{1,0:T(8,128)(2,1)S(1)}, bf16[16,1024]{1,0:T(8,128)(2,1)}, u32[]{:S(2)}) copy-start(bf16[16,1024]{1,0:T(8,128)(2,1)} %param.12) | copy-start | bytes 98308
  7.2 94.7 %copy-start.3 = (f32[1024]{0:T(1024)S(1)}, f32[1024]{0:T(1024)}, u32[]{:S(2)}) copy-start(f32[1024]{0:T(1024)} %param.21) | copy-start | bytes 12292
  7.2 44.4 %all-reduce.13.cloned.1.call-start = ((), (), s32[]{:S(2)}) async-start(), calls=%async_computation.3 | async-start | bytes 262144
  14.1 86.9 %all-reduce.7.cloned.1.call-start = ((), (), s32[]{:S(2)}) async-start(), calls=%async_computation | async-start | bytes 131072 | tf_op jit(solution)/shard_map/psum | solution.py:71
  54.3 52.9 %copy-start.1 = (f32[4,4,128,128]{3,2,1,0:T(8,128)}, f32[4,4,128,128]{3,2,1,0:T(8,128)S(1)}, u32[]{:S(2)}) copy-start(f32[4,4,128,128]{3,2,1,0:T(8,128)S(1)} %multiply_add_fusion) | copy-start | bytes 3145732
  69.6 73.4 %all-reduce.9.cloned.1.call-start = ((), (), s32[]{:S(2)}) async-start(), calls=%async_computation.1 | async-start | bytes 524288 | tf_op jit(solution)/shard_map/psum | solution.py:76
  107.2 72.7 %all-reduce.11.cloned.1.call-start = ((), (), s32[]{:S(2)}) async-start(), calls=%async_computation.2 | async-start | bytes 131072 | tf_op jit(solution)/shard_map/psum | solution.py:80
Sparse Core Ops, SparseCore 0:
  14.2 37.3 all-reduce.12
  69.7 31.1 all-reduce.6
  107.4 35.5 all-reduce.8
  148.5 31.3 all-reduce.10
where the time goes:
time: 189 us; the launch traced here: 188 us
  waiting for transfers between devices  107 us (57%)
  blocking collectives  38.5 us (20%)
  matrix products  18.6 us (10%)
  between operations  14.5 us (8%)
  other arithmetic  7.69 us (4%)
    psum x1, waiting for transfers between devices, shards(): layer_out = (middle + lax.psum(down_terms, 'tp')).astype(jnp.bfloat16)  31.6 us
    psum x1, waiting for transfers between devices, shards(): mixed = (inputs + lax.psum(head_terms, 'tp')).astype(jnp.bfloat16)  31.3 us
    psum x1, waiting for transfers between devices, shards(): up_full, total_sq2 = lax.psum((upward, squares2), 'kv')  23.9 us
    unnamed x5, waiting for transfers between devices  20.4 us
    unnamed x1, blocking collectives  13.5 us
    all_gather x1, blocking collectives, shards(): lax.all_gather(retained, 'kv', axis=0, tiled=True)  13.2 us
    psum x1, blocking collectives, shards(): up_full, total_sq2 = lax.psum((upward, squares2), 'kv')  11.8 us
    dot_general x4, matrix products, shards(): jnp.dot(normed, weight, preferred_element_type=jnp.float32)  6.11 us
  transfers between devices with their start and end apart: 4, of which 4 were waited for; matrix products, arithmetic and copies ran while one was open for 2% of the time, Pallas kernels for 0%

commit v1 on v0

--- a/solution.py
+++ b/solution.py
@@ -68,7 +68,7 @@
         w_out,
         preferred_element_type=jnp.float32,
     )
-    mixed = (inputs + lax.psum(head_terms, "tp")).astype(jnp.bfloat16)
+    mixed = (inputs + jnp.sum(lax.all_gather(head_terms, "tp"), axis=0)).astype(jnp.bfloat16)
     middle = mixed.astype(jnp.float32)
     squares2 = jnp.sum(middle * middle, axis=1)
     normed2 = (middle * mlp_gain).astype(jnp.bfloat16)

time: 189 us -> 161 us (0.85)
  waiting for transfers between devices: 107 us -> 76.6 us
  blocking collectives: 38.5 us -> 43 us
    psum x1 -> x0, waiting for transfers between devices: 31.3 us -> none  [shards(): mixed = (inputs + lax.psum(head_terms, 'tp')).astype(jnp.bfloat16)]
    all_gather x0 -> x1, blocking collectives: none -> 5.77 us  [shards(): lax.all_gather(head_terms, 'tp')]
    unnamed x5 -> x4, waiting for transfers between devices: 20.4 us -> 20.4 us
  transfers between devices with their start and end apart: 4 -> 3, of which waited for: 4 -> 3; matrix products, arithmetic and copies ran while one was open for 2% -> 2% of each run, Pallas kernels for 0% -> 0%
where the time goes in v1:
time: 161 us; the launch traced here: 160 us
  waiting for transfers between devices  76.6 us (48%)
  blocking collectives  43 us (27%)
  matrix products  18 us (11%)
  between operations  14.5 us (9%)
  other arithmetic  6.87 us (4%)
    psum x1, waiting for transfers between devices, shards(): layer_out = (middle + lax.psum(down_terms, 'tp')).astype(jnp.bfloat16)  31.6 us
    psum x1, waiting for transfers between devices, shards(): up_full, total_sq2 = lax.psum((upward, squares2), 'kv')  24.7 us
    unnamed x4, waiting for transfers between devices  20.4 us
    unnamed x1, blocking collectives  13.5 us
    all_gather x1, blocking collectives, shards(): lax.all_gather(retained, 'kv', axis=0, tiled=True)  13.2 us
    psum x1, blocking collectives, shards(): up_full, total_sq2 = lax.psum((upward, squares2), 'kv')  10.5 us
    dot_general x4, matrix products, shards(): jnp.dot(normed, weight, preferred_element_type=jnp.float32)  6.11 us
    all_gather x1, blocking collectives, shards(): lax.all_gather(head_terms, 'tp')  5.77 us
  transfers between devices with their start and end apart: 3, of which 3 were waited for; matrix products, arithmetic and copies ran while one was open for 2% of the time, Pallas kernels for 0%

profile of v1, /device:TPU:0, one launch (start us, length us, event | category | flops | bytes accessed | tf_op | source)
XLA Modules:
  0.0 160.4 jit_solution(15602884767458923079)
XLA Ops:
  7.2 0.0 all-reduce.10.cloned.1.call-start
  7.2 1.6 convolution_bitcast_fusion.3
  8.8 1.5 convolution_bitcast_fusion.2
  10.3 1.5 convolution_bitcast_fusion.1
  11.8 1.5 convolution_bitcast_fusion
  13.4 0.7 pad_maximum_fusion
  14.1 0.0 all-reduce.6.cloned.1.call-start
  14.1 0.9 fusion.4
  15.0 0.7 convert_element_type.40
  15.7 0.1 multiply_cosine_fusion
  15.8 1.2 dynamic-slice
  17.7 13.5 %all-reduce.1 = f32[16]{0:T(128)S(1)} all-reduce(f32[16]{0:T(128)S(1)} %fusion.4), channel_id=4, replica_groups=mesh['grp'=2,'kv'=4,'tp'=4] {'kv'}, use_global_device_ids=true, to_apply=%region_2.0.clone | all-reduce | flops 16 | bytes 128
  31.2 0.1 fusion.19
  31.3 20.3 %all-reduce.10.cloned.1.call-done = f32[16,4,512]{2,0,1:T(8,128)} async-done(((f32[16,4,512]{2,0,1:T(8,128)}), f32[16,4,512]{2,0,1:T(8,128)}) %all-reduce.10.cloned.1.call-update) | async-done | bytes 131088
  51.6 0.9 dynamic-slice_multiply_fusion
  52.5 0.1 multiply_subtract_fusion
  52.6 0.1 pad_maximum_fusion.1
  52.7 1.6 multiply_add_fusion
  54.3 1.0 fusion.22
  55.3 0.1 multiply_reduce_fusion
  55.4 0.1 fusion.17
  55.5 13.2 %all-gather.1 = bf16[4,4,512]{2,1,0:T(4,128)(2,1)S(1)} all-gather(bf16[1,4,512]{2,1,0:T(4,128)(2,1)S(1)} %reshape.109), channel_id=1, replica_groups=mesh['grp'=2,'kv'=4,'tp'=4] {'kv'}, dimensions={0}, use_global_device_ids=true | all-gather | bytes 20480 | tf_op jit(solution)/shard_map/all_gather | solution.py:67
  68.7 0.3 fusion.23
  68.9 5.8 %all-gather = f32[64,1024]{1,0:T(8,128)S(1)} all-gather(f32[16,1024]{1,0:T(8,128)S(1)} %fusion.23), channel_id=2, replica_groups=mesh['grp'=2,'kv'=4,'tp'=4] {'tp'}, dimensions={0}, use_global_device_ids=true | all-gather | bytes 327680 | tf_op jit(solution)/shard_map/all_gather | solution.py:71
  74.7 0.1 fusion.7
  74.9 5.3 %fusion.9 = f32[16,4096]{1,0:T(8,128)} fusion(bf16[1024,4096]{1,0:T(8,128)(2,1)} %param.22, bf16[16,1024]{1,0:T(8,128)(2,1)S(1)} %get-tuple-element.3, f32[1024]{0:T(1024)S(1)} %copy-done.3), kind=kOutput, calls=%fused_computation.22 | convolution fusion | flops 134266880 | bytes 8687616 | tf_op jit(solution)/shard_map/dot_general | solution.py:75
  80.2 0.0 all-reduce.8.cloned.1.call-start
  80.2 10.5 %psum.22 = f32[16]{0:T(128)S(1)} all-reduce(f32[16]{0:T(128)S(1)} %get-tuple-element.2), channel_id=1, replica_groups=mesh['grp'=2,'kv'=4,'tp'=4] {'kv'}, use_global_device_ids=true, to_apply=%region_7.8 | all-reduce | flops 16 | bytes 128 | tf_op jit(solution)/shard_map/psum | solution.py:76
  90.8 24.7 %all-reduce.6.cloned.1.call-done = f32[16,4096]{1,0:T(8,128)} async-done(((f32[16,4096]{1,0:T(8,128)}), f32[16,4096]{1,0:T(8,128)}) %all-reduce.6.cloned.1.call-update) | async-done | bytes 262160 | tf_op jit(solution)/shard_map/psum | solution.py:76
  115.5 5.3 %fusion = f32[16,1024]{1,0:T(8,128)} fusion(bf16[4096,1024]{1,0:T(8,128)(2,1)} %param.23, f32[16,4096]{1,0:T(8,128)} %all-reduce.6.cloned.1.call-done, f32[16]{0:T(128)S(1)} %add_rsqrt_fusion.1), kind=kOutput, calls=%fused_computation.6 | convolution fusion | flops 134479872 | bytes 8716352 | tf_op jit(solution)/shard_map/dot_general | solution.py:79
  120.8 31.6 %all-reduce.8.cloned.1.call-done = f32[16,1024]{1,0:T(8,128)} async-done(((f32[16,1024]{1,0:T(8,128)}), f32[16,1024]{1,0:T(8,128)}) %all-reduce.8.cloned.1.call-update) | async-done | bytes 65552 | tf_op jit(solution)/shard_map/psum | solution.py:80
  152.4 1.5 fusion.8
  (20 shorter events, 0.2 us)
Async XLA Ops:
  7.2 61.5 %copy-start = (bf16[512,1024]{1,0:T(8,128)(2,1)S(1)}, bf16[512,1024]{1,0:T(8,128)(2,1)}, u32[]{:S(2)}) copy-start(bf16[512,1024]{1,0:T(8,128)(2,1)} %param.20) | copy-start | bytes 3145732
  7.2 67.6 %copy-start.2 = (bf16[16,1024]{1,0:T(8,128)(2,1)S(1)}, bf16[16,1024]{1,0:T(8,128)(2,1)}, u32[]{:S(2)}) copy-start(bf16[16,1024]{1,0:T(8,128)(2,1)} %param.12) | copy-start | bytes 98308
  7.2 67.7 %copy-start.3 = (f32[1024]{0:T(1024)S(1)}, f32[1024]{0:T(1024)}, u32[]{:S(2)}) copy-start(f32[1024]{0:T(1024)} %param.21) | copy-start | bytes 12292
  7.2 44.4 %all-reduce.10.cloned.1.call-start = ((), (), s32[]{:S(2)}) async-start(), calls=%async_computation.2 | async-start | bytes 262144
  14.1 101.4 %all-reduce.6.cloned.1.call-start = ((), (), s32[]{:S(2)}) async-start(), calls=%async_computation | async-start | bytes 524288 | tf_op jit(solution)/shard_map/psum | solution.py:76
  54.3 25.9 %copy-start.1 = (f32[4,4,128,128]{3,2,1,0:T(8,128)}, f32[4,4,128,128]{3,2,1,0:T(8,128)S(1)}, u32[]{:S(2)}) copy-start(f32[4,4,128,128]{3,2,1,0:T(8,128)S(1)} %multiply_add_fusion) | copy-start | bytes 3145732
  80.2 72.2 %all-reduce.8.cloned.1.call-start = ((), (), s32[]{:S(2)}) async-start(), calls=%async_computation.1 | async-start | bytes 131072 | tf_op jit(solution)/shard_map/psum | solution.py:80
Sparse Core Ops, SparseCore 0:
  14.2 37.3 all-reduce.9
  80.3 35.0 all-reduce.5
  120.9 31.3 all-reduce.7
